TPU v7x, 32 devices: a whole 2x2x4 slice. The times are simulated.
32 devices in a mesh: sp: 8 (over z, x), tp: 4 (over y, core).
Axes of the slice: x: 2, y: 2, z: 4, core: 2. Of those that a mesh axis runs over, the one named last changes fastest.
Arguments:
- tokens: bfloat16 [8192, 4096], P('sp'), may hold values from -6 to 6
- input_norm_scale: bfloat16 [4096], replicated, may hold values from 0.099609375 to 1.8984375
- mean_input_weight: bfloat16 [4096, 2048], P('sp', 'tp'), may hold values from -0.09375 to 0.09375
- query_matrix: bfloat16 [4096, 2048], P('sp', 'tp'), may hold values from -0.09375 to 0.09375
- key_matrix: bfloat16 [4096, 2048], P('sp', 'tp'), may hold values from -0.09375 to 0.09375
- value_matrix: bfloat16 [4096, 2048], P('sp', 'tp'), may hold values from -0.09375 to 0.09375
- strength_weight: bfloat16 [4096, 16], P('sp', 'tp'), may hold values from -0.09375 to 0.09375
- decay_input_weight: bfloat16 [4096, 16], P('sp', 'tp'), may hold values from -0.25 to 0.25
- causal_filter_weight: bfloat16 [4, 3, 2048], replicated, may hold values from -3 to 3
- head_decay_logrates: float32 [16], replicated, may hold values from -13.2 to -2.9
- decay_input_shift: float32 [16], replicated, may hold values from -1 to 1
- strength_shift: float32 [16], replicated, may hold values from -5 to -3
- decay_spike: float32 [8192, 16], P('sp', 'tp'), may hold values from -1.3 to 0
- head_norm_scale: bfloat16 [128], replicated, may hold values from 0.099609375 to 1.8984375
- group_mixing_weight: bfloat16 [16, 128, 128], replicated, may hold values from -0.5 to 0.5
- mean_channel_scale: bfloat16 [2048], replicated, may hold values from 0.099609375 to 1.8984375
- mean_output_weight: bfloat16 [2048, 4096], P('tp', 'sp'), may hold values from -0.09375 to 0.09375
- delta_output_weight: bfloat16 [2048, 4096], P('tp', 'sp'), may hold values from -0.09375 to 0.09375
Outputs:
- mixed_out: bfloat16 [8192, 4096], P(('sp', 'tp'))
All inputs are finite; a program needn't handle non-finite values.
Results may differ from a plain program's by a relative error of at most 0.015.
Values may be sent and summed in bfloat16 or wider, within the bound.
No kernel may reach another device: no remote copies, remote signals or barrier semaphores. Data moves between devices by JAX's collectives and lax.ppermute only.
A program may use at most 128 MiB of HBM per device.

v0:
```python
import jax
import jax.numpy as jnp
from jax import lax
from jax.sharding import PartitionSpec as P

GROUP_DIM = 128
HEAD_DIM = 128
CONV = 4
BLOCK = 64


EPSILON = 1e-06


def shifted_2(block, axis, distance):
    devices = range(lax.axis_size(axis))
    route = [(i - distance, i) for i in devices if i - distance in devices]
    return lax.ppermute(block, axis, route)


def scale_rows(values, gain_vec):
    squares = jnp.mean(values * values, axis=-1, keepdims=True)
    return values * lax.rsqrt(squares + EPSILON) * gain_vec.astype(jnp.float32)


def unit_rows(values):
    return values * lax.rsqrt(jnp.sum(values * values, axis=-1, keepdims=True) + EPSILON)


def causal_taps(extended, taps, rows_out):
    tap_sum = jnp.zeros((rows_out, taps.shape[1]), jnp.float32)
    for tap_index in range(taps.shape[0]):
        tap_sum = tap_sum + taps[tap_index] * extended[tap_index : tap_index + rows_out]
    return jax.nn.silu(tap_sum)


def pool_means(previous, current, group_ids, positions):
    pool_reach = 15
    rows_out = current.shape[0]
    extended = jnp.concatenate([previous, current], axis=0).astype(jnp.float32)
    window_size = jnp.left_shift(jnp.int32(2), group_ids % 4)
    windowed = jnp.zeros(current.shape, jnp.float32)
    for lag_rows in range(pool_reach + 1):
        shifted = extended[pool_reach - lag_rows : pool_reach - lag_rows + rows_out]
        windowed = windowed + jnp.where(lag_rows < window_size[None, :], shifted, 0.0)
    counts = jnp.minimum(positions[:, None] + 1, window_size[None, :]).astype(jnp.float32)
    return (windowed / counts - extended[pool_reach:]).astype(jnp.bfloat16)


def unit_lower_solve(strict_part, right_side):
    power = strict_part
    solved = right_side - jnp.einsum(
        "nhij,nhjd->nhid", power, right_side, precision=lax.Precision.HIGHEST
    )
    for square_index in range((BLOCK - 1).bit_length() - 1):
        power = jnp.einsum("nhij,nhjk->nhik", power, power, precision=lax.Precision.HIGHEST)
        solved = solved + jnp.einsum(
            "nhij,nhjd->nhid", power, solved, precision=lax.Precision.HIGHEST
        )
    return solved


def block_terms(query, keys, values, decay_logarithm, beta):
    blocks = keys.shape[0] // BLOCK

    def to_blocks(tensor):
        return jnp.swapaxes(tensor.reshape((blocks, BLOCK) + tensor.shape[1:]), 1, 2)

    query_b = to_blocks(query)
    keys_b = to_blocks(keys)
    values_b = to_blocks(values)
    decay_b = to_blocks(decay_logarithm)
    beta_b = to_blocks(beta)
    cumulative = jnp.cumsum(decay_b, axis=-1)
    positions = jnp.arange(BLOCK)
    causal = positions[:, None] >= positions[None, :]
    strict = positions[:, None] > positions[None, :]
    spread = cumulative[..., :, None] - cumulative[..., None, :]
    weights = jnp.where(causal, jnp.exp(jnp.where(causal, spread, 0.0)), 0.0)
    keys_beta = keys_b * beta_b[..., None]
    values_beta = values_b * beta_b[..., None]
    intersection = jnp.einsum("nhid,nhjd->nhij", keys_beta, keys_b, precision=lax.Precision.HIGHEST)
    strict_part = jnp.where(strict, intersection * weights, 0.0)
    right_side = jnp.concatenate([values_beta, keys_beta * jnp.exp(cumulative)[..., None]], axis=-1)
    solved = unit_lower_solve(strict_part, right_side)
    value_depth = values.shape[-1]
    update = solved[..., :value_depth]
    project = solved[..., value_depth:]
    scores = (
        jnp.einsum("nhid,nhjd->nhij", query_b, keys_b, precision=lax.Precision.HIGHEST) * weights
    )
    query_dec = query_b * jnp.exp(cumulative)[..., None]
    keys_dec = keys_b * jnp.exp(cumulative[..., -1:] - cumulative)[..., None]
    carry_decay = jnp.exp(cumulative[..., -1])
    return (scores, query_dec, keys_dec, update, project, carry_decay)


def run_blocks(state, terms):

    def advance(carried, inputs):
        scores, query_dec, keys_dec, update, project, carry_decay = inputs
        fresh = update - jnp.einsum(
            "hcd,hde->hce", project, carried, precision=lax.Precision.HIGHEST
        )
        output = jnp.einsum("hcd,hde->hce", query_dec, carried, precision=lax.Precision.HIGHEST)
        output = output + jnp.einsum("hij,hje->hie", scores, fresh, precision=lax.Precision.HIGHEST)
        carried = carried * carry_decay[:, None, None] + jnp.einsum(
            "hcd,hce->hde", keys_dec, fresh, precision=lax.Precision.HIGHEST
        )
        return (carried, output)

    final_state, outputs = lax.scan(advance, state, terms)
    return outputs


def apply_map(step_map, target):
    return jnp.einsum("hde,hef->hdf", step_map, target, precision=lax.Precision.HIGHEST)


def block_maps(terms, head_count, head_depth):
    scores, query_dec, keys_dec, update, project, carry_decay = terms
    identity = jnp.eye(head_depth, dtype=jnp.float32)
    step_maps = carry_decay[..., None, None] * identity - jnp.einsum(
        "nhcd,nhce->nhde", keys_dec, project, precision=lax.Precision.HIGHEST
    )
    injects = jnp.einsum("nhcd,nhce->nhde", keys_dec, update, precision=lax.Precision.HIGHEST)

    def compose(carried, inputs):
        step_map, inject = inputs
        return ((apply_map(step_map, carried[0]), apply_map(step_map, carried[1]) + inject), None)

    start_maps = (
        jnp.broadcast_to(identity, (head_count, head_depth, head_depth)),
        jnp.zeros((head_count, head_depth, head_depth), jnp.float32),
    )
    composed, unused = lax.scan(compose, start_maps, (step_maps, injects))
    return composed


def per_device(
    tokens,
    input_norm_scale,
    mean_input_weight,
    query_matrix,
    key_matrix,
    value_matrix,
    strength_weight,
    decay_input_weight,
    causal_filter_weight,
    head_decay_logrates,
    decay_input_shift,
    strength_shift,
    decay_spike,
    head_norm_scale,
    group_mixing_weight,
    mean_channel_scale,
    mean_output_weight,
    delta_output_weight,
):
    tok_rows = tokens.shape[0]
    pool_cols = mean_input_weight.shape[1]
    delta_cols = query_matrix.shape[1]
    head_count = strength_weight.shape[1]
    head_depth = delta_cols // head_count
    groups_dev = pool_cols // GROUP_DIM
    tp_index = lax.axis_index("tp")
    sp_index = lax.axis_index("sp")
    normed = scale_rows(tokens.astype(jnp.float32), input_norm_scale).astype(jnp.bfloat16)
    pieces = (
        lax.all_gather(mean_input_weight, "sp", axis=0, tiled=True),
        lax.all_gather(query_matrix, "sp", axis=0, tiled=True),
        lax.all_gather(key_matrix, "sp", axis=0, tiled=True),
        lax.all_gather(value_matrix, "sp", axis=0, tiled=True),
        lax.all_gather(strength_weight, "sp", axis=0, tiled=True),
        lax.all_gather(decay_input_weight, "sp", axis=0, tiled=True),
    )
    wide_part = jnp.concatenate(pieces[:4], axis=1)
    narrow_part = jnp.concatenate(pieces[4:], axis=1)
    wide_sum = jnp.dot(normed, wide_part, preferred_element_type=jnp.float32)
    narrow_sum = jnp.dot(normed, narrow_part, preferred_element_type=jnp.float32)
    pool_raw = wide_sum[:, :pool_cols].astype(jnp.bfloat16)
    qkv_raw = wide_sum[:, pool_cols:].astype(jnp.bfloat16)
    beta_raw = narrow_sum[:, :head_count].astype(jnp.bfloat16)
    decay_unshaped = narrow_sum[:, head_count:].astype(jnp.bfloat16)
    pool_reach = 15
    conv_reach = CONV - 1
    previous_pool, previous_qkv = shifted_2(
        (pool_raw[tok_rows - pool_reach :], qkv_raw[tok_rows - conv_reach :]), "sp", 1
    )
    conv_local = (
        lax.dynamic_slice_in_dim(causal_filter_weight, tp_index * delta_cols, delta_cols, 2)
        .reshape(CONV, 3 * delta_cols)
        .astype(jnp.float32)
    )
    extended_qkv = jnp.concatenate([previous_qkv, qkv_raw], axis=0).astype(jnp.float32)
    convolved = causal_taps(extended_qkv, conv_local, tok_rows)
    query = unit_rows(
        convolved[:, :delta_cols].reshape(tok_rows, head_count, head_depth)
    ) * HEAD_DIM ** (-0.5)
    keys = unit_rows(
        convolved[:, delta_cols : 2 * delta_cols].reshape(tok_rows, head_count, head_depth)
    )
    values = convolved[:, 2 * delta_cols :].reshape(tok_rows, head_count, head_depth)
    rate_logarithm = lax.dynamic_slice_in_dim(
        head_decay_logrates, tp_index * head_count, head_count
    )
    shift_amounts = lax.dynamic_slice_in_dim(decay_input_shift, tp_index * head_count, head_count)
    strength_offsets = lax.dynamic_slice_in_dim(strength_shift, tp_index * head_count, head_count)
    beta = jax.nn.sigmoid(beta_raw.astype(jnp.float32) + strength_offsets)
    decay_logarithm = (
        -jnp.exp(rate_logarithm)
        * jax.nn.softplus(decay_unshaped.astype(jnp.float32) + shift_amounts)
        + decay_spike
    )
    terms = block_terms(query, keys, values, decay_logarithm, beta)
    transfer_map, offset_map = block_maps(terms, head_count, head_depth)

    def hop(step_count, incoming):
        advanced = apply_map(transfer_map, incoming) + offset_map
        return shifted_2(advanced.astype(jnp.bfloat16), "sp", 1).astype(advanced.dtype)

    incoming = lax.fori_loop(0, lax.axis_size("sp") - 1, hop, jnp.zeros_like(offset_map))
    outputs = run_blocks(incoming, terms)
    delta_rows = jnp.swapaxes(outputs, 1, 2).reshape(tok_rows, head_count, head_depth)
    delta_mixed = (
        scale_rows(delta_rows, head_norm_scale).astype(jnp.bfloat16).reshape(tok_rows, delta_cols)
    )
    group_ids = tp_index * groups_dev + jnp.arange(pool_cols) // GROUP_DIM
    positions = sp_index * tok_rows + jnp.arange(tok_rows)
    pool_diff = pool_means(previous_pool, pool_raw, group_ids, positions)
    local_mix = lax.dynamic_slice_in_dim(group_mixing_weight, tp_index * groups_dev, groups_dev, 0)
    pooled = jnp.einsum(
        "tgc,gcd->tgd",
        pool_diff.reshape(tok_rows, groups_dev, GROUP_DIM),
        local_mix,
        preferred_element_type=jnp.float32,
    )
    pool_scale = lax.dynamic_slice_in_dim(mean_channel_scale, tp_index * pool_cols, pool_cols)
    pool_mixed = (pooled.reshape(tok_rows, pool_cols) * pool_scale.astype(jnp.float32)).astype(
        jnp.bfloat16
    )
    mixed = jnp.concatenate([pool_mixed, delta_mixed], axis=1)
    pool_weight_rows, delta_weight_rows = (
        lax.all_gather(mean_output_weight, "sp", axis=1, tiled=True),
        lax.all_gather(delta_output_weight, "sp", axis=1, tiled=True),
    )
    out_weight = jnp.concatenate([pool_weight_rows, delta_weight_rows], axis=0)
    return lax.psum_scatter(
        jnp.dot(mixed, out_weight, preferred_element_type=jnp.float32).astype(jnp.bfloat16),
        "tp",
        scatter_dimension=0,
        tiled=True,
    )


def solution(mesh):
    return jax.shard_map(
        per_device,
        mesh=mesh,
        in_specs=(
            P("sp", None),
            P(),
            P("sp", "tp"),
            P("sp", "tp"),
            P("sp", "tp"),
            P("sp", "tp"),
            P("sp", "tp"),
            P("sp", "tp"),
            P(),
            P(),
            P(),
            P(),
            P("sp", "tp"),
            P(),
            P(),
            P(),
            P("tp", "sp"),
            P("tp", "sp"),
        ),
        out_specs=P(("sp", "tp"), None),
        check_vma=False,
    )
```

profile of v0, /device:TPU:0, one launch (start us, length us, event | category | flops | bytes accessed | tf_op | source)
XLA Modules:
  0.0 758.3 jit_solution(1002801814942155716)
XLA Ops:
  16.0 5.3 fusion.32
  21.3 33.6 %all_gather.28 = bf16[4096,4]{0,1:T(4,128)(2,1)S(1)} all-gather(bf16[512,4]{0,1:T(4,128)(2,1)S(1)} %copy-done.11), channel_id=1, replica_groups=mesh['sp'=8,'tp'=4] {'sp'}, dimensions={0}, use_global_device_ids=true | all-gather | bytes 36864 | tf_op jit(solution)/shard_map/all_gather | solution.py:174
  55.0 31.6 %all_gather.29 = bf16[4096,4]{0,1:T(4,128)(2,1)S(1)} all-gather(bf16[512,4]{0,1:T(4,128)(2,1)S(1)} %copy-done.12), channel_id=1, replica_groups=mesh['sp'=8,'tp'=4] {'sp'}, dimensions={0}, use_global_device_ids=true | all-gather | bytes 36864 | tf_op jit(solution)/shard_map/all_gather | solution.py:175
  86.6 2.4 fusion.104
  92.6 66.7 %all-gather.13.cloned.1.call-done = bf16[4096,512]{1,0:T(8,128)(2,1)} async-done(((bf16[512,512]{1,0:T(8,128)(2,1)}), bf16[4096,512]{1,0:T(8,128)(2,1)}) %all-gather.13.cloned.1.call-update) | async-done | bytes 4194320 | tf_op jit(solution)/shard_map/all_gather | solution.py:173
  159.3 73.5 %all-gather.7.cloned.1.call-done = bf16[4096,512]{1,0:T(8,128)(2,1)} async-done(((bf16[512,512]{1,0:T(8,128)(2,1)}), bf16[4096,512]{1,0:T(8,128)(2,1)}) %all-gather.7.cloned.1.call-update) | async-done | bytes 4194320 | tf_op jit(solution)/shard_map/all_gather | solution.py:170
  232.7 73.3 %all-gather.9.cloned.1.call-done = bf16[4096,512]{1,0:T(8,128)(2,1)} async-done(((bf16[512,512]{1,0:T(8,128)(2,1)}), bf16[4096,512]{1,0:T(8,128)(2,1)}) %all-gather.9.cloned.1.call-update) | async-done | bytes 4194320 | tf_op jit(solution)/shard_map/all_gather | solution.py:171
  306.1 27.1 %fusion.53 = bf16[1024,2048]{1,0:T(8,128)(2,1)} fusion(bf16[4096,512]{1,0:T(8,128)(2,1)} %all-gather.13.cloned.1.call-done, bf16[4096,512]{1,0:T(8,128)(2,1)} %all-gather.11.cloned.1.call-done, bf16[4096,512]{1,0:T(8,128)(2,1)} %all-gather.9.cloned.1.call-done, bf16[4096,512]{1,0:T(8,128)(2,1)} %all-gather.7.cloned.1.call-done, ...), kind=kOutput, calls=%fused_computation.66 | convolution fusion | flops 17265852416 | bytes 29380608 | tf_op jit(solution)/shard_map/dot_general | solution.py:179
  333.9 2.5 collective-permute-start.2
  337.3 2.2 copy-done.1
  340.1 5.0 collective-permute-start.1
  346.1 3.7 divide_multiply_fusion
  349.9 4.5 slice_multiply_fusion.4
  354.4 1.9 mul.252
  356.4 2.0 reduce_sum.37
  359.7 1.9 reshape.220
  361.6 3.7 mul.264
  365.3 3.6 reduce_sum.38
  368.9 1.9 add_rsqrt_fusion
  372.0 2.9 reshape.222
  375.0 3.1 reshape_reshape.3
  378.1 4.6 multiply_select_fusion
  382.7 2.3 fusion.143
  385.0 2.4 fusion.144
  387.4 5.5 fusion.93
  392.9 7.3 multiply_multiply_fusion
  400.2 4.3 fusion.57
  404.5 4.8 convolution_add_fusion.6
  409.3 2.4 fusion.146
  411.7 4.7 fusion.145
  416.4 2.3 fusion.147
  418.8 4.8 convolution_add_fusion.5
  423.6 2.3 fusion.149
  425.9 4.5 fusion.148
  430.4 4.8 convolution_add_fusion.4
  435.2 2.6 fusion.141
  437.9 8.5 %fusion.138 = f32[16,4,128,128]{3,2,1,0:T(8,128)} fusion(f32[16,4,64,128]{3,2,1,0:T(8,128)S(1)} %get-tuple-element.411, f32[16,4,64,256]{3,2,1,0:T(8,128)S(1)} %convolution_add_fusion.4), kind=kOutput, calls=%fused_computation.210 | convolution fusion | flops 805306368 | bytes 8388608 | tf_op jit(solution)/shard_map/nhcd,nhce->nhde/dot_general | solution.py:126
  446.4 8.8 %multiply_subtract_fusion = f32[16,4,128,128]{3,2,1,0:T(8,128)} fusion(f32[16,4,64,128]{3,2,1,0:T(8,128)S(1)} %get-tuple-element.411, f32[128,128]{1,0:T(8,128)S(1)} %fusion.120, f32[16,4]{1,0:T(8,128)S(1)} %copy.88, f32[16,4,64,256]{3,2,1,0:T(8,128)S(1)} %convolution_add_fusion.4), kind=kOutput, calls=%fused_computation.65 | convolution fusion | flops 807403520 | bytes 8462336 | tf_op jit(solution)/shard_map/nhcd,nhce->nhde/dot_general | solution.py:123
  455.2 45.7 %while.37 = (s32[]{:T(128)}, f32[4,128,128]{2,1,0:T(8,128)S(1)}, f32[4,128,128]{2,1,0:T(8,128)S(1)}, f32[16,4,128,128]{3,2,1,0:T(8,128)}, f32[16,4,128,128]{3,2,1,0:T(8,128)}, /*index=5*/s32[]{:T(128)}, s32[]{:T(128)}) while((s32[]{:T(128)}, f32[4,128,128]{2,1,0:T(8,128)S(1)}, f32[4,128,128]{2,1,0:T(8,128)S(1)}, ...), condition=%wide.region_4.5_spmd.clone, body=%wide.region_3.4_spmd.clone.sunk | while | flops 201457664 | bytes 2885207 | solution.py:136
  501.0 61.3 %while.38 = (s32[]{:T(128)}, f32[4,128,128]{2,1,0:T(8,128)S(1)}, f32[4,128,128]{2,1,0:T(8,128)S(1)}, f32[4,128,128]{2,1,0:T(8,128)S(1)}, s32[]{:T(128)}, /*index=5*/s32[]{:T(128)}) while((s32[]{:T(128)}, f32[4,128,128]{2,1,0:T(8,128)S(1)}, f32[4,128,128]{2,1,0:T(8,128)S(1)}, f32[4,128,128]{2,1,0:T(8,128)S(1)}, s32[]{:T(128)}, ...), condition=%wide.region_6.7_spmd.clone, body=%wide.region_5.6_spmd.clone.sunk | while | flops 100925440 | bytes 1835127 | solution.py:222
  501.4 2.6 collective-permute-start
  507.2 5.1 collective-permute-start
  515.5 5.6 collective-permute-start
  524.2 6.0 collective-permute-start
  533.4 6.0 collective-permute-start
  539.5 2.2 collective-permute-done
  543.0 6.3 collective-permute-start
  549.3 3.1 collective-permute-done
  553.7 5.8 collective-permute-start
  562.3 81.5 %while.36 = (s32[]{:T(128)}, f32[4,128,128]{2,1,0:T(8,128)S(1)}, f32[16,4,64,128]{3,2,1,0:T(8,128)}, f32[16,4]{1,0:T(8,128)S(1)}, f32[16,4,64,128]{3,2,1,0:T(8,1...) while((s32[]{:T(128)}, f32[4,128,128]{2,1,0:T(8,128)S(1)}, ...), condition=%wide.region_9.10_spmd, body=%wide.region_8.9_spmd.sunk | while | flops 176357376 | bytes 2493581 | solution.py:112
  564.8 1.9 fusion.207
  580.0 1.9 fusion.207
  585.1 1.9 fusion.207
  595.3 1.9 fusion.207
  600.4 1.9 fusion.207
  610.5 1.9 fusion.207
  620.7 1.9 fusion.207
  625.8 1.9 fusion.207
  635.9 1.9 fusion.207
  643.8 2.4 multiply_reduce_fusion
  652.1 8.1 %fusion.107 = f32[4,128,1024]{2,1,0:T(8,128)} fusion(bf16[16,128,128]{2,1,0:T(8,128)(2,1)S(1)} %copy-done, s32[]{:T(128)S(6)} %select_n.189, s32[512]{0:T(512)S(1)} %copy-done.13, s32[1024]{0:T(1024)S(1)} %add_add_fusion, f32[1039,512]{1,0:T(8,128)S(1)} %maximum_convert_fusion.1, pred[512]{0:T(512)(128)(4,1)S(1)} %copy-done.18, ...), kind=kOutput, calls=%fused_computation.135 | convolution fusion | flops 153092096 | bytes 35796996 | tf_op jit(solution)/shard_map/tgc,gcd->tgd/dot_general | solution.py:232
  660.2 1.9 copy.87
  663.4 13.8 %fusion.47 = bf16[1024,4096]{1,0:T(8,128)(2,1)} fusion(bf16[512,4096]{1,0:T(8,128)(2,1)} %all-gather.17.cloned.1.call-done, bf16[512,4096]{1,0:T(8,128)(2,1)} %all-gather.15.cloned.1.call-done, bf16[1024,512]{1,0:T(8,128)(2,1)} %fusion.67, bf16[1024,512]{1,0:T(8,128)(2,1)} %multiply_convert_fusion), kind=kOutput, calls=%fused_computation.55 | convolution fusion | flops 8615100416 | bytes 18874368 | tf_op jit(solution)/shard_map/dot_general | solution.py:249
  677.3 73.7 %reduce-scatter.2.cloned.1.call-done = bf16[256,4096]{1,0:T(8,128)(2,1)} async-done(((bf16[1024,4096]{1,0:T(8,128)(2,1)}), bf16[256,4096]{1,0:T(8,128)(2,1)}) %reduce-scatter.2.cloned.1.call-update) | async-done | bytes 2097168 | tf_op jit(solution)/shard_map/reduce_scatter | solution.py:248
  (299 shorter events, 152.3 us)
Async XLA Ops:
  6.5 645.4 %copy-start = (bf16[16,128,128]{2,1,0:T(8,128)(2,1)S(1)}, bf16[16,128,128]{2,1,0:T(8,128)(2,1)}, u32[]{:S(2)}) copy-start(bf16[16,128,128]{2,1,0:T(8,128)(2,1)} %param.38) | copy-start | bytes 1572868
  6.5 9.2 %copy-start.14 = (f32[16]{0:T(128)S(1)}, f32[16]{0:T(128)}, u32[]{:S(2)}) copy-start(f32[16]{0:T(128)} %param.34) | copy-start | bytes 196
  6.5 9.3 %copy-start.15 = (f32[16]{0:T(128)S(1)}, f32[16]{0:T(128)}, u32[]{:S(2)}) copy-start(f32[16]{0:T(128)} %param.35) | copy-start | bytes 196
  6.5 9.4 %copy-start.16 = (f32[16]{0:T(128)S(1)}, f32[16]{0:T(128)}, u32[]{:S(2)}) copy-start(f32[16]{0:T(128)} %param.33) | copy-start | bytes 196
  6.5 9.5 %copy-start.8 = (bf16[4096]{0:T(1024)(128)(2,1)S(1)}, bf16[4096]{0:T(1024)(128)(2,1)}, u32[]{:S(2)}) copy-start(bf16[4096]{0:T(1024)(128)(2,1)} %param.25) | copy-start | bytes 24580
  6.5 86.0 %all-gather.11.cloned.1.call-start = ((), (), s32[]{:S(2)}) async-start(), calls=%async_computation.3 | async-start | bytes 4718592 | tf_op jit(solution)/shard_map/all_gather | solution.py:172
  7.3 152.0 %all-gather.13.cloned.1.call-start = ((), (), s32[]{:S(2)}) async-start(), calls=%async_computation.4 | async-start | bytes 4718592 | tf_op jit(solution)/shard_map/all_gather | solution.py:173
  8.0 224.7 %all-gather.7.cloned.1.call-start = ((), (), s32[]{:S(2)}) async-start(), calls=%async_computation.1 | async-start | bytes 4718592 | tf_op jit(solution)/shard_map/all_gather | solution.py:170
  8.8 297.3 %all-gather.9.cloned.1.call-start = ((), (), s32[]{:S(2)}) async-start(), calls=%async_computation.2 | async-start | bytes 4718592 | tf_op jit(solution)/shard_map/all_gather | solution.py:171
  9.3 654.1 %all-gather.15.cloned.1.call-start = ((), (), s32[]{:S(2)}) async-start(), calls=%async_computation.5 | async-start | bytes 4718592 | tf_op jit(solution)/shard_map/all_gather | solution.py:244
  9.9 653.5 %all-gather.17.cloned.1.call-start = ((), (), s32[]{:S(2)}) async-start(), calls=%async_computation.6 | async-start | bytes 4718592 | tf_op jit(solution)/shard_map/all_gather | solution.py:245
  10.5 740.5 %reduce-scatter.2.cloned.1.call-start = ((), (), s32[]{:S(2)}) async-start(), calls=%async_computation.7 | async-start | bytes 10485760 | tf_op jit(solution)/shard_map/reduce_scatter | solution.py:248
  16.0 5.3 copy-start.11
  16.0 39.0 %copy-start.12 = (bf16[512,4]{0,1:T(4,128)(2,1)S(1)}, bf16[512,4]{0,1:T(4,128)(2,1)}, u32[]{:S(2)}) copy-start(bf16[512,4]{0,1:T(4,128)(2,1)} %param.31) | copy-start | bytes 12292
  16.0 70.6 %copy-start.5 = (bf16[1024,4096]{1,0:T(8,128)(2,1)S(1)}, bf16[1024,4096]{1,0:T(8,128)(2,1)}, u32[]{:S(2)}) copy-start(bf16[1024,4096]{1,0:T(8,128)(2,1)} %param.24) | copy-start | bytes 25165828
  86.6 2.4 copy-start.7
  86.6 4.6 copy-start.17
  333.9 11.2 %collective-permute-start.2 = (bf16[3,1536]{1,0:T(4,128)(2,1)S(1)}, bf16[3,1536]{1,0:T(4,128)(2,1)S(1)}, u32[]{:S(2)}, u32[]{:S(2)}) collective-permute-start(bf16[3,1536]{1,0:T(4,128)(2,1)S(1)} %slice.177), channel_id=1, source_target_pairs={{0,4},{4,8},{8,12},{12,16},{16,20},{20,24},{24,28},{1,5},{5,9},{9,... | collective-permute-start | bytes 27656 | tf_op jit(solution)/shard_map/ppermute | solution.py:18
  337.3 2.2 copy-start.1
  337.3 7.8 %slice-start = ((bf16[1024,2048]{1,0:T(8,128)(2,1)}), bf16[1024,1536]{1,0:T(8,128)(2,1)S(1)}, s32[]{:S(2)}) async-start(bf16[1024,2048]{1,0:T(8,128)(2,1)} %fusion.53), calls=%async_computation.8 | async-start | bytes 6291456 | tf_op jit(solution)/shard_map/slice | solution.py:182
  340.1 310.7 %collective-permute-start.1 = (bf16[15,512]{1,0:T(8,128)(2,1)}, bf16[15,512]{1,0:T(8,128)(2,1)}, u32[]{:S(2)}, u32[]{:S(2)}) collective-permute-start(bf16[15,512]{1,0:T(8,128)(2,1)} %slice.156), channel_id=1, source_target_pairs={{0,4},{4,8},{8,12},{12,16},{16,20},{20,24},{24,28},{1,5},{5,9},{9,... | collective-permute-start | bytes 46088 | tf_op jit(solution)/shard_map/ppermute | solution.py:18
  361.6 25.8 %copy-start.2 = (f32[16,64,4,128]{3,2,1,0:T(4,128)}, f32[16,64,4,128]{3,2,1,0:T(4,128)S(1)}, u32[]{:S(2)}) copy-start(f32[16,64,4,128]{3,2,1,0:T(4,128)S(1)} %reshape.220) | copy-start | bytes 6291460
  374.9 3.1 copy-start.9
  385.0 2.4 copy-start.3
  387.4 5.5 copy-start.4
  501.4 4.4 collective-permute-start
  507.2 7.0 collective-permute-start
  515.5 7.4 collective-permute-start
  524.2 7.9 %collective-permute-start = (bf16[4,128,128]{2,1,0:T(8,128)(2,1)S(1)}, bf16[4,128,128]{2,1,0:T(8,128)(2,1)}, u32[]{:S(2)}, u32[]{:S(2)}) collective-permute-start(bf16[4,128,128]{2,1,0:T(8,128)(2,1)S(1)} %fusion.215), channel_id=1, source_target_pairs={{0,4},{4,8},{8,12},{12,16},{16,20},{20,24},{24,28},{1,5},{5,9},{9,... | collective-permute-start | bytes 393224 | tf_op jit(solution)/shard_map/while/body/eval_jaxpr/ppermute | solution.py:18
  533.4 8.2 %collective-permute-start = (bf16[4,128,128]{2,1,0:T(8,128)(2,1)S(1)}, bf16[4,128,128]{2,1,0:T(8,128)(2,1)}, u32[]{:S(2)}, u32[]{:S(2)}) collective-permute-start(bf16[4,128,128]{2,1,0:T(8,128)(2,1)S(1)} %fusion.215), channel_id=1, source_target_pairs={{0,4},{4,8},{8,12},{12,16},{16,20},{20,24},{24,28},{1,5},{5,9},{9,... | collective-permute-start | bytes 393224 | tf_op jit(solution)/shard_map/while/body/eval_jaxpr/ppermute | solution.py:18
  543.0 9.5 %collective-permute-start = (bf16[4,128,128]{2,1,0:T(8,128)(2,1)S(1)}, bf16[4,128,128]{2,1,0:T(8,128)(2,1)}, u32[]{:S(2)}, u32[]{:S(2)}) collective-permute-start(bf16[4,128,128]{2,1,0:T(8,128)(2,1)S(1)} %fusion.215), channel_id=1, source_target_pairs={{0,4},{4,8},{8,12},{12,16},{16,20},{20,24},{24,28},{1,5},{5,9},{9,... | collective-permute-start | bytes 393224 | tf_op jit(solution)/shard_map/while/body/eval_jaxpr/ppermute | solution.py:18
  553.7 7.6 %collective-permute-start = (bf16[4,128,128]{2,1,0:T(8,128)(2,1)S(1)}, bf16[4,128,128]{2,1,0:T(8,128)(2,1)}, u32[]{:S(2)}, u32[]{:S(2)}) collective-permute-start(bf16[4,128,128]{2,1,0:T(8,128)(2,1)S(1)} %fusion.215), channel_id=1, source_target_pairs={{0,4},{4,8},{8,12},{12,16},{16,20},{20,24},{24,28},{1,5},{5,9},{9,... | collective-permute-start | bytes 393224 | tf_op jit(solution)/shard_map/while/body/eval_jaxpr/ppermute | solution.py:18
  643.8 2.6 copy-start.6
  649.1 1.7 slice-start.1
  650.7 1.2 copy-start.13
  650.7 1.2 copy-start.18
  650.7 1.2 copy-start.19
  650.7 1.2 copy-start.20
  650.7 1.2 copy-start.21
  650.7 1.2 copy-start.22
  650.8 1.2 copy-start.23
  650.8 1.2 copy-start.24
  650.8 1.2 copy-start.25
  650.8 1.2 copy-start.26
  650.8 1.2 copy-start.27
  650.8 1.2 copy-start.28
  650.8 1.2 copy-start.29
  650.8 1.2 copy-start.30
  650.8 1.2 copy-start.31
  650.8 1.2 copy-start.32
  650.9 1.2 copy-start.33
  660.2 1.9 copy-start.10
Sparse Core Ops, SparseCore 0:
  9.5 76.2 all-gather.10
  87.9 71.2 all-gather.12
  161.4 71.3 all-gather.6
  234.7 71.3 all-gather.8
  308.0 73.5 all-gather.14
  383.5 72.8 all-gather.16
  677.4 73.5 reduce-scatter.1
where the time goes:
time: 769 us; the launch traced here: 758 us
  waiting for transfers between devices  305 us (40%)
  matrix products  246 us (32%)
  blocking collectives  65.2 us (8%)
  other arithmetic  52.1 us (7%)
  starting transfers between devices  45.1 us (6%)
  local copies, waits for them, and re-layouts  27.6 us (4%)
  between operations  14.7 us (2%)
    reduce_scatter x1, waiting for transfers between devices, per_device(): lax.psum_scatter(jnp.dot(mixed, out_weight, preferred_element_type=jnp.fl...  73.7 us
    all_gather x1, waiting for transfers between devices, per_device(): lax.all_gather(mean_input_weight, 'sp', axis=0, tiled=True)  73.5 us
    all_gather x1, waiting for transfers between devices, per_device(): lax.all_gather(query_matrix, 'sp', axis=0, tiled=True)  73.3 us
    all_gather x1, waiting for transfers between devices, per_device(): lax.all_gather(value_matrix, 'sp', axis=0, tiled=True)  66.7 us
    dot_general x39, matrix products, apply_map(): jnp.einsum('hde,hef->hdf', step_map, target, precision=lax.Precision.HIGH...  47.1 us
    ppermute x9, starting transfers between devices, shifted_2(): return lax.ppermute(block, axis, route)  44.8 us
    all_gather x1, blocking collectives, per_device(): lax.all_gather(strength_weight, 'sp', axis=0, tiled=True)  33.6 us
    all_gather x1, blocking collectives, per_device(): lax.all_gather(decay_input_weight, 'sp', axis=0, tiled=True)  31.6 us
  transfers between devices with their start and end apart: 16, of which 11 were waited for; matrix products, arithmetic and copies ran while one was open for 41% of the time, Pallas kernels for 0%

commit v1 on v0

v1 whole, which is shorter than its diff:
```python
import jax
import jax.numpy as jnp
from jax import lax
from jax.experimental import pallas as pl
from jax.experimental.pallas import tpu as pltpu
from jax.sharding import PartitionSpec as P

GROUP_DIM = 128
HEAD_DIM = 128
CONV = 4
CHUNK = 128


EPSILON = 1e-06


def shifted_2(block, axis, distance):
    devices = range(lax.axis_size(axis))
    route = [(i - distance, i) for i in devices if i - distance in devices]
    return lax.ppermute(block, axis, route)


def scale_rows(values, gain_vec):
    squares = jnp.mean(values * values, axis=-1, keepdims=True)
    return values * lax.rsqrt(squares + EPSILON) * gain_vec.astype(jnp.float32)


def unit_rows(values):
    return values * lax.rsqrt(jnp.sum(values * values, axis=-1, keepdims=True) + EPSILON)


def causal_taps(extended, taps, rows_out):
    tap_sum = jnp.zeros((rows_out, taps.shape[1]), jnp.float32)
    for tap_index in range(taps.shape[0]):
        tap_sum = tap_sum + taps[tap_index] * extended[tap_index : tap_index + rows_out]
    return jax.nn.silu(tap_sum)


def pool_means(previous, current, group_ids, positions):
    pool_reach = 15
    rows_out = current.shape[0]
    extended = jnp.concatenate([previous, current], axis=0).astype(jnp.float32)
    window_size = jnp.left_shift(jnp.int32(2), group_ids % 4)
    windowed = jnp.zeros(current.shape, jnp.float32)
    for lag_rows in range(pool_reach + 1):
        shifted = extended[pool_reach - lag_rows : pool_reach - lag_rows + rows_out]
        windowed = windowed + jnp.where(lag_rows < window_size[None, :], shifted, 0.0)
    counts = jnp.minimum(positions[:, None] + 1, window_size[None, :]).astype(jnp.float32)
    return (windowed / counts - extended[pool_reach:]).astype(jnp.bfloat16)


def mxu(left, right, left_dim, right_dim):
    return lax.dot_general(
        left.astype(jnp.bfloat16),
        right.astype(jnp.bfloat16),
        (((left_dim,), (right_dim,)), ((), ())),
        preferred_element_type=jnp.float32,
    )


def delta_kernel(raw_ref, halo_ref, taps_ref, gates_ref, local_ref, reach_ref, maps_ref, ext_ref):
    chunk = raw_ref.shape[0]
    heads, depth = maps_ref.shape[0], maps_ref.shape[1]
    width = heads * depth
    pad = halo_ref.shape[0]
    conv = taps_ref.shape[0]
    step = pl.program_id(0)
    rows = lax.broadcasted_iota(jnp.int32, (chunk, chunk), 0)
    cols = lax.broadcasted_iota(jnp.int32, (chunk, chunk), 1)

    @pl.when(step == 0)
    def _():
        ext_ref[:pad] = halo_ref[...].astype(jnp.float32)
        lane = lax.broadcasted_iota(jnp.int32, (depth, 2 * depth), 1)
        sub = lax.broadcasted_iota(jnp.int32, (depth, 2 * depth), 0)
        for h in range(heads):
            maps_ref[h] = jnp.where(lane == sub, 1.0, 0.0)

    @pl.when(step > 0)
    def _():
        ext_ref[:pad] = ext_ref[chunk : chunk + pad]

    ext_ref[pad:] = raw_ref[...].astype(jnp.float32)

    def taps_of(part, h):
        low = part * width + h * depth
        total = jnp.zeros((chunk, depth), jnp.float32)
        for i in range(conv):
            first = pad - conv + 1 + i
            total = total + (
                taps_ref[i : i + 1, low : low + depth]
                * ext_ref[first : first + chunk, low : low + depth]
            )
        return total / (1.0 + jnp.exp(-total))

    gates = gates_ref[...]
    causal = rows >= cols
    cumul = lax.dot_general(
        jnp.where(causal, 1.0, 0.0),
        gates,
        (((1,), (0,)), ((), ())),
        precision=lax.Precision.HIGHEST,
        preferred_element_type=jnp.float32,
    )
    cumul_t = cumul.T
    hs = range(heads)
    lower, scores, rights, query_dec, keys_dec, carry = [], [], [], [], [], []
    for h in hs:
        query = unit_rows(taps_of(0, h)) * depth ** (-0.5)
        keys = unit_rows(taps_of(1, h))
        values = taps_of(2, h)
        beta = gates[:, heads + h : heads + h + 1]
        cum = cumul[:, h : h + 1]
        last = cum[chunk - 1 :, :]
        weights = jnp.exp(jnp.where(causal, cum - cumul_t[h : h + 1, :], -1e30))
        keys_16 = keys.astype(jnp.bfloat16)
        lower.append(
            jnp.where(rows > cols, mxu(keys_16, keys_16, 1, 1) * (weights * beta), 0.0)
        )
        scores.append((mxu(query, keys_16, 1, 1) * weights).astype(jnp.bfloat16))
        grown = jnp.exp(cum)
        keys_beta = keys * beta
        rights.append(
            jnp.concatenate([keys_beta * grown, values * beta], axis=1).astype(jnp.bfloat16)
        )
        query_dec.append(query * grown)
        keys_dec.append((keys * jnp.exp(last - cum)).astype(jnp.bfloat16))
        carry.append(jnp.exp(last))
    lower_16 = [x.astype(jnp.bfloat16) for x in lower]
    span = 1
    differ = jnp.bitwise_xor(rows, cols)
    inverse = [jnp.where(rows == cols, 1.0, jnp.where(differ == 1, -x, 0.0)) for x in lower]
    span = 2
    while span < chunk:
        level = jnp.logical_and(differ >= span, differ < 2 * span)
        inner = [
            mxu(jnp.where(level, lower_16[h], jnp.zeros_like(lower_16[h])), inverse[h], 1, 0)
            for h in hs
        ]
        inverse = [inverse[h] - mxu(inverse[h], inner[h], 1, 0) for h in hs]
        span *= 2
    solved = [mxu(inverse[h], rights[h], 1, 0).astype(jnp.bfloat16) for h in hs]
    mixed = [mxu(scores[h], solved[h], 1, 0) for h in hs]
    injects = [mxu(keys_dec[h], solved[h], 0, 0) for h in hs]
    before = [maps_ref[h] for h in hs]
    before_16 = [x.astype(jnp.bfloat16) for x in before]
    reach = [mxu(query_dec[h] - mixed[h][:, :depth], before_16[h], 1, 0) for h in hs]
    moved = [mxu(injects[h][:, :depth], before_16[h], 1, 0) for h in hs]
    for h in hs:
        low = h * depth
        local_ref[:, low : low + depth] = mixed[h][:, depth:] + reach[h][:, depth:]
        reach_ref[:, low : low + depth] = reach[h][:, :depth].astype(jnp.bfloat16)
        after = before[h] * carry[h] - moved[h]
        maps_ref[h, :, :depth] = after[:, :depth]
        maps_ref[h, :, depth:] = after[:, depth:] + injects[h][:, depth:]


def delta_local(raw, halo, taps, gates, heads, depth):
    tok_rows, wide = raw.shape
    chunk = min(CHUNK, tok_rows)
    width = heads * depth
    return pl.pallas_call(
        delta_kernel,
        grid=(tok_rows // chunk,),
        in_specs=[
            pl.BlockSpec((chunk, wide), lambda i: (i, 0)),
            pl.BlockSpec(halo.shape, lambda i: (0, 0)),
            pl.BlockSpec(taps.shape, lambda i: (0, 0)),
            pl.BlockSpec((chunk, gates.shape[1]), lambda i: (i, 0)),
        ],
        out_specs=[
            pl.BlockSpec((chunk, width), lambda i: (i, 0)),
            pl.BlockSpec((chunk, width), lambda i: (i, 0)),
            pl.BlockSpec((heads, depth, 2 * depth), lambda i: (0, 0, 0)),
        ],
        out_shape=[
            jax.ShapeDtypeStruct((tok_rows, width), jnp.float32),
            jax.ShapeDtypeStruct((tok_rows, width), jnp.bfloat16),
            jax.ShapeDtypeStruct((heads, depth, 2 * depth), jnp.float32),
        ],
        scratch_shapes=[pltpu.VMEM((chunk + halo.shape[0], wide), jnp.float32)],
        compiler_params=pltpu.CompilerParams(dimension_semantics=("arbitrary",)),
        cost_estimate=pl.CostEstimate(
            flops=60 * tok_rows * width * chunk, bytes_accessed=10 * tok_rows * width, transcendentals=0
        ),
    )(raw, halo, taps, gates)


def finish_kernel(place_ref, maps_ref, local_ref, reach_ref, gain_ref, out_ref, state_ref):
    count, heads, depth = maps_ref.shape[0], maps_ref.shape[1], maps_ref.shape[2]

    @pl.when(pl.program_id(0) == 0)
    def _():
        place = place_ref[0]
        states = [jnp.zeros((depth, depth), jnp.float32) for h in range(heads)]
        for j in range(count - 1):
            for h in range(heads):
                found = maps_ref[j, h]
                moved = mxu(found[:, :depth], states[h], 1, 0) + found[:, depth:].astype(jnp.float32)
                states[h] = jnp.where(j < place, moved, states[h])
        for h in range(heads):
            state_ref[h] = states[h].astype(jnp.bfloat16)

    for h in range(heads):
        low = h * depth
        rows = local_ref[:, low : low + depth] + mxu(
            reach_ref[:, low : low + depth], state_ref[h], 1, 0
        )
        out_ref[:, low : low + depth] = scale_rows(rows, gain_ref[...]).astype(jnp.bfloat16)


def delta_finish(place, maps, local, reach, gain):
    tok_rows, width = local.shape
    heads, depth = maps.shape[1], maps.shape[2]
    block = min(256, tok_rows)
    return pl.pallas_call(
        finish_kernel,
        grid=(tok_rows // block,),
        in_specs=[
            pl.BlockSpec(memory_space=pltpu.SMEM),
            pl.BlockSpec(maps.shape, lambda i: (0, 0, 0, 0)),
            pl.BlockSpec((block, width), lambda i: (i, 0)),
            pl.BlockSpec((block, width), lambda i: (i, 0)),
            pl.BlockSpec((1, depth), lambda i: (0, 0)),
        ],
        out_specs=pl.BlockSpec((block, width), lambda i: (i, 0)),
        out_shape=jax.ShapeDtypeStruct((tok_rows, width), jnp.bfloat16),
        scratch_shapes=[pltpu.VMEM((heads, depth, depth), jnp.bfloat16)],
        compiler_params=pltpu.CompilerParams(dimension_semantics=("arbitrary",)),
        cost_estimate=pl.CostEstimate(
            flops=4 * tok_rows * width * depth, bytes_accessed=8 * tok_rows * width, transcendentals=0
        ),
    )(place, maps, local, reach, gain)


def per_device(
    tokens,
    input_norm_scale,
    mean_input_weight,
    query_matrix,
    key_matrix,
    value_matrix,
    strength_weight,
    decay_input_weight,
    causal_filter_weight,
    head_decay_logrates,
    decay_input_shift,
    strength_shift,
    decay_spike,
    head_norm_scale,
    group_mixing_weight,
    mean_channel_scale,
    mean_output_weight,
    delta_output_weight,
):
    tok_rows = tokens.shape[0]
    pool_cols = mean_input_weight.shape[1]
    delta_cols = query_matrix.shape[1]
    head_count = strength_weight.shape[1]
    head_depth = delta_cols // head_count
    groups_dev = pool_cols // GROUP_DIM
    tp_index = lax.axis_index("tp")
    sp_index = lax.axis_index("sp")
    normed = scale_rows(tokens.astype(jnp.float32), input_norm_scale).astype(jnp.bfloat16)
    narrow_own = jnp.concatenate([strength_weight, decay_input_weight], axis=1).T
    narrow_part = lax.all_gather(narrow_own, "sp", axis=1, tiled=True)
    qkv_raw = jnp.concatenate(
        [
            jnp.dot(
                normed,
                lax.all_gather(own, "sp", axis=0, tiled=True),
                preferred_element_type=jnp.float32,
            ).astype(jnp.bfloat16)
            for own in (query_matrix, key_matrix, value_matrix)
        ],
        axis=1,
    )
    pool_raw = jnp.dot(
        normed,
        lax.all_gather(mean_input_weight, "sp", axis=0, tiled=True),
        preferred_element_type=jnp.float32,
    ).astype(jnp.bfloat16)
    narrow_sum = mxu(normed, narrow_part, 1, 1)
    beta_raw = narrow_sum[:, :head_count].astype(jnp.bfloat16)
    decay_unshaped = narrow_sum[:, head_count:].astype(jnp.bfloat16)
    pool_reach = 15
    previous_qkv = shifted_2(qkv_raw[tok_rows - 8 :], "sp", 1)
    previous_pool = shifted_2(pool_raw[tok_rows - pool_reach :], "sp", 1)
    conv_local = (
        lax.dynamic_slice_in_dim(causal_filter_weight, tp_index * delta_cols, delta_cols, 2)
        .reshape(CONV, 3 * delta_cols)
        .astype(jnp.float32)
    )
    rate_logarithm = lax.dynamic_slice_in_dim(
        head_decay_logrates, tp_index * head_count, head_count
    )
    shift_amounts = lax.dynamic_slice_in_dim(decay_input_shift, tp_index * head_count, head_count)
    strength_offsets = lax.dynamic_slice_in_dim(strength_shift, tp_index * head_count, head_count)
    beta = jax.nn.sigmoid(beta_raw.astype(jnp.float32) + strength_offsets)
    decay_logarithm = (
        -jnp.exp(rate_logarithm)
        * jax.nn.softplus(decay_unshaped.astype(jnp.float32) + shift_amounts)
        + decay_spike
    )
    gates = jnp.concatenate([decay_logarithm, beta], axis=1)
    gates = jnp.pad(gates, ((0, 0), (0, 128 - 2 * head_count)))
    local_rows, reach, own_maps = delta_local(
        qkv_raw, previous_qkv, conv_local, gates, head_count, head_depth
    )
    maps = lax.all_gather(own_maps.astype(jnp.bfloat16), "sp", axis=0)
    delta_mixed = delta_finish(
        sp_index.reshape(1), maps, local_rows, reach, head_norm_scale.reshape(1, -1)
    )
    group_ids = tp_index * groups_dev + jnp.arange(pool_cols) // GROUP_DIM
    positions = sp_index * tok_rows + jnp.arange(tok_rows)
    pool_diff = pool_means(previous_pool, pool_raw, group_ids, positions)
    local_mix = lax.dynamic_slice_in_dim(group_mixing_weight, tp_index * groups_dev, groups_dev, 0)
    pooled = jnp.einsum(
        "tgc,gcd->tgd",
        pool_diff.reshape(tok_rows, groups_dev, GROUP_DIM),
        local_mix,
        preferred_element_type=jnp.float32,
    )
    pool_scale = lax.dynamic_slice_in_dim(mean_channel_scale, tp_index * pool_cols, pool_cols)
    pool_mixed = (pooled.reshape(tok_rows, pool_cols) * pool_scale.astype(jnp.float32)).astype(
        jnp.bfloat16
    )
    pool_out = jnp.dot(
        pool_mixed,
        lax.all_gather(mean_output_weight, "sp", axis=1, tiled=True),
        preferred_element_type=jnp.float32,
    )
    delta_out = jnp.dot(
        delta_mixed,
        lax.all_gather(delta_output_weight, "sp", axis=1, tiled=True),
        preferred_element_type=jnp.float32,
    )
    return lax.psum_scatter(
        (pool_out + delta_out).astype(jnp.bfloat16), "tp", scatter_dimension=0, tiled=True
    )


def solution(mesh):
    return jax.shard_map(
        per_device,
        mesh=mesh,
        in_specs=(
            P("sp", None),
            P(),
            P("sp", "tp"),
            P("sp", "tp"),
            P("sp", "tp"),
            P("sp", "tp"),
            P("sp", "tp"),
            P("sp", "tp"),
            P(),
            P(),
            P(),
            P(),
            P("sp", "tp"),
            P(),
            P(),
            P(),
            P("tp", "sp"),
            P("tp", "sp"),
        ),
        out_specs=P(("sp", "tp"), None),
        check_vma=False,
    )
```

time: 769 us -> 599 us (0.78); the launches traced: 758 us -> 599 us
  matrix products: 246 us -> 73.5 us
  waiting for transfers between devices: 305 us -> 413 us
  starting transfers between devices: 45.1 us -> 5.69 us
  Pallas kernels: 0 us -> 35.2 us
  other arithmetic: 52.1 us -> 19.7 us
  blocking collectives: 65.2 us -> 33.5 us
  local copies, waits for them, and re-layouts: 27.6 us -> 4.19 us
    dot_general x121 -> x7, matrix products: 238 us -> 67.6 us  [the longest x3 27.1 us: per_device(): jnp.dot(normed, lax.all_gather(own, 'sp', axis=0, tiled=True), preferred_...]
    all_gather x1, waiting for transfers between devices: 0.01 us -> 69 us  [per_device(): lax.all_gather(delta_output_weight, 'sp', axis=1, tiled=True)]
    all_gather x1, waiting for transfers between devices: 0.01 us -> 55.9 us  [per_device(): lax.all_gather(mean_output_weight, 'sp', axis=1, tiled=True)]
    all_gather x1, waiting for transfers between devices: 73.5 us -> 24.9 us  [per_device(): lax.all_gather(mean_input_weight, 'sp', axis=0, tiled=True)]
    all_gather x3 -> x4, waiting for transfers between devices: 140 us -> 188 us  [the longest x3 149 us: per_device(): lax.all_gather(own, 'sp', axis=0, tiled=True)]
    ppermute x9 -> x2, starting transfers between devices: 44.8 us -> 5.41 us  [shifted_2(): return lax.ppermute(block, axis, route)]
    pallas_call x0 -> x2, Pallas kernels: none -> 35.2 us  [the longest x1 29 us: delta_local(): pl.pallas_call(delta_kernel, grid=(tok_rows // chunk,), in_specs=[pl.Bloc...]
    all_gather x2 -> x1, blocking collectives: 65.2 us -> 33.5 us  [per_device(): narrow_part = lax.all_gather(narrow_own, 'sp', axis=1, tiled=True)]
  transfers between devices with their start and end apart: 16 -> 10, of which waited for: 11 -> 9; matrix products, arithmetic and copies ran while one was open for 41% -> 13% of each run, Pallas kernels for 0% -> 6%
where the time goes in v1:
time: 599 us
  waiting for transfers between devices  413 us (69%)
  matrix products  73.5 us (12%)
  Pallas kernels  35.2 us (6%)
  blocking collectives  33.5 us (6%)
  other arithmetic  19.7 us (3%)
  between operations  13.7 us (2%)
    all_gather x3, waiting for transfers between devices, per_device(): lax.all_gather(own, 'sp', axis=0, tiled=True)  149 us
    reduce_scatter x1, waiting for transfers between devices, per_device(): lax.psum_scatter((pool_out + delta_out).astype(jnp.bfloat16), 'tp', scatt...  69.8 us
    all_gather x1, waiting for transfers between devices, per_device(): lax.all_gather(delta_output_weight, 'sp', axis=1, tiled=True)  69 us
    all_gather x1, waiting for transfers between devices, per_device(): lax.all_gather(mean_output_weight, 'sp', axis=1, tiled=True)  55.9 us
    all_gather x1, waiting for transfers between devices, per_device(): maps = lax.all_gather(own_maps.astype(jnp.bfloat16), 'sp', axis=0)  38.8 us
    all_gather x1, blocking collectives, per_device(): narrow_part = lax.all_gather(narrow_own, 'sp', axis=1, tiled=True)  33.5 us
    pallas_call x1, Pallas kernels, delta_local(): pl.pallas_call(delta_kernel, grid=(tok_rows // chunk,), in_specs=[pl.Bloc...  29 us
    dot_general x3, matrix products, per_device(): jnp.dot(normed, lax.all_gather(own, 'sp', axis=0, tiled=True), preferred_...  27.1 us
  transfers between devices with their start and end apart: 10, of which 9 were waited for; matrix products, arithmetic and copies ran while one was open for 13% of the time, Pallas kernels for 6%

profile of v1, /device:TPU:0, one launch (start us, length us, event | category | flops | bytes accessed | tf_op | source)
XLA Modules:
  0.0 598.6 jit_solution(3615770280701173312)
XLA Ops:
  6.5 0.7 all-gather.17.cloned.1.call-update
  7.3 0.0 all-gather.15.cloned.1.call-start
  7.3 0.7 all-gather.15.cloned.1.call-update
  8.0 0.0 all-gather.13.cloned.1.call-start
  8.1 0.7 all-gather.13.cloned.1.call-update
  8.7 0.0 all-gather.9.cloned.1.call-start
  8.8 0.5 all-gather.9.cloned.1.call-update
  9.3 0.0 all-gather.11.cloned.1.call-start
  9.4 0.5 all-gather.11.cloned.1.call-update
  9.9 0.0 all-gather.21.cloned.1.call-start
  10.0 5.1 fusion
  15.1 0.0 copy-start.8
  15.1 0.0 copy-start.9
  15.1 0.0 copy-start.5
  15.1 0.0 copy-start.6
  15.1 0.0 copy-start.10
  15.1 10.4 %fusion.2 = bf16[1024,4096]{1,0:T(8,128)(2,1)} fusion(bf16[1024,4096]{1,0:T(8,128)(2,1)} %param.18, f32[4096]{0:T(1024)S(1)} %convert_element_type.58, f32[1024]{0:T(1024)S(1)} %add_rsqrt_fusion), kind=kLoop, calls=%fused_computation.4 | loop fusion | flops 16777216 | bytes 16797696 | tf_op jit(solution)/shard_map/convert_element_type | solution.py:264
  25.5 0.0 copy-done.8
  25.5 0.1 dynamic_slice.22
  25.6 0.0 copy-done.9
  25.6 0.1 dynamic_slice.23
  25.7 33.5 %all_gather.32 = bf16[8,4096]{1,0:T(8,128)(2,1)S(1)} all-gather(bf16[8,512]{1,0:T(8,128)(2,1)S(1)} %maximum_bitcast_fusion), channel_id=1, replica_groups=mesh['sp'=8,'tp'=4] {'sp'}, dimensions={1}, use_global_device_ids=true | all-gather | bytes 73728 | tf_op jit(solution)/shard_map/all_gather | solution.py:266
  59.3 0.0 copy-done.10
  59.3 0.1 exponential_negate_fusion
  59.3 5.7 convolution_convert_fusion.4
  65.0 0.1 fusion.28
  65.2 20.4 %all-gather.17.cloned.1.call-done = bf16[4096,512]{1,0:T(8,128)(2,1)} async-done(((bf16[512,512]{1,0:T(8,128)(2,1)}), bf16[4096,512]{1,0:T(8,128)(2,1)}) %all-gather.17.cloned.1.call-update) | async-done | bytes 4194320 | tf_op jit(solution)/shard_map/all_gather | solution.py:271
  85.6 9.0 %convolution_convert_fusion = bf16[1024,512]{1,0:T(8,128)(2,1)S(1)} fusion(bf16[1024,4096]{1,0:T(8,128)(2,1)} %fusion.2, bf16[4096,512]{1,0:T(8,128)(2,1)} %all-gather.17.cloned.1.call-done), kind=kOutput, calls=%fused_computation.42 | convolution fusion | flops 4295491584 | bytes 13631488 | tf_op jit(solution)/shard_map/dot_general | solution.py:269
  94.6 64.6 %all-gather.15.cloned.1.call-done = bf16[4096,512]{1,0:T(8,128)(2,1)} async-done(((bf16[512,512]{1,0:T(8,128)(2,1)}), bf16[4096,512]{1,0:T(8,128)(2,1)}) %all-gather.15.cloned.1.call-update) | async-done | bytes 4194320 | tf_op jit(solution)/shard_map/all_gather | solution.py:271
  159.2 9.0 %convolution_convert_fusion.1 = bf16[1024,512]{1,0:T(8,128)(2,1)S(1)} fusion(bf16[1024,4096]{1,0:T(8,128)(2,1)} %fusion.2, bf16[4096,512]{1,0:T(8,128)(2,1)} %all-gather.15.cloned.1.call-done), kind=kOutput, calls=%fused_computation.43 | convolution fusion | flops 4295491584 | bytes 13631488 | tf_op jit(solution)/shard_map/dot_general | solution.py:269
  168.3 64.4 %all-gather.13.cloned.1.call-done = bf16[4096,512]{1,0:T(8,128)(2,1)} async-done(((bf16[512,512]{1,0:T(8,128)(2,1)}), bf16[4096,512]{1,0:T(8,128)(2,1)}) %all-gather.13.cloned.1.call-update) | async-done | bytes 4194320 | tf_op jit(solution)/shard_map/all_gather | solution.py:271
  232.7 9.0 %convolution_convert_fusion.2 = bf16[1024,512]{1,0:T(8,128)(2,1)S(1)} fusion(bf16[1024,4096]{1,0:T(8,128)(2,1)} %fusion.2, bf16[4096,512]{1,0:T(8,128)(2,1)} %all-gather.13.cloned.1.call-done), kind=kOutput, calls=%fused_computation.44 | convolution fusion | flops 4295491584 | bytes 13631488 | tf_op jit(solution)/shard_map/dot_general | solution.py:269
  241.8 0.3 pad_maximum_fusion.raw_ref
  242.0 1.6 copy-done.2
  243.7 2.7 collective-permute-start.1
  246.4 0.7 constant_dynamic-slice_fusion
  247.1 0.2 copy.51
  247.3 0.6 convert.6.taps_ref
  247.9 0.8 pad.4.gates_ref
  248.7 0.0 collective-permute-done.1.halo_ref
  248.7 0.6 copy-done.7
  249.3 29.0 %shard_map.172 = (f32[1024,512]{1,0:T(8,128)}, bf16[1024,512]{1,0:T(8,128)(2,1)}, f32[4,128,256]{2,1,0:T(8,128)}) custom-call(bf16[1024,1536]{1,0:T(8,128)(2,1)} %copy-done.2, bf16[8,1536]{1,0:T(8,128)(2,1)} %copy-done.7, f32[4,1536]{1,0:T(4,128)} %convert.6.taps_ref, f32[1024,128]{1,0:T(8,128)} %pad.4.gates_ref), custom_call_target="tpu_custom_call" | custom-call | flops 4026531840 | bytes 5242880 | tf_op jit(solution)/shard_map/pallas_call | solution.py:162
  278.3 1.8 convert_element_type.73
  280.1 0.0 all-gather.21.cloned.1.call-update
  280.1 0.0 all-gather.19.cloned.1.call-start
  280.1 0.7 all-gather.19.cloned.1.call-update
  280.8 0.0 reduce-scatter.2.cloned.1.call-start
  281.0 0.8 dynamic-slice_convert_fusion
  281.8 24.9 %all-gather.9.cloned.1.call-done = bf16[4096,512]{1,0:T(8,128)(2,1)} async-done(((bf16[512,512]{1,0:T(8,128)(2,1)}), bf16[4096,512]{1,0:T(8,128)(2,1)}) %all-gather.9.cloned.1.call-update) | async-done | bytes 4194320 | tf_op jit(solution)/shard_map/all_gather | solution.py:280
  306.7 9.0 %convolution_convert_fusion.3 = bf16[1024,512]{1,0:T(8,128)(2,1)S(1)} fusion(bf16[1024,4096]{1,0:T(8,128)(2,1)} %fusion.2, bf16[4096,512]{1,0:T(8,128)(2,1)} %all-gather.9.cloned.1.call-done), kind=kOutput, calls=%fused_computation.45 | convolution fusion | flops 4295491584 | bytes 13631488 | tf_op jit(solution)/shard_map/dot_general | solution.py:278
  315.7 2.7 collective-permute-start
  318.5 1.4 collective-permute-done
  319.9 0.3 maximum_convert_fusion
  320.2 0.0 copy-done
  320.2 5.9 fusion.22
  326.2 0.2 fusion.20
  326.3 55.9 %all-gather.11.cloned.1.call-done = bf16[512,4096]{1,0:T(8,128)(2,1)} async-done(((bf16[512,512]{1,0:T(8,128)(2,1)}), bf16[512,4096]{1,0:T(8,128)(2,1)}) %all-gather.11.cloned.1.call-update) | async-done | bytes 4194320 | tf_op jit(solution)/shard_map/all_gather | solution.py:330
  382.3 10.5 %fusion.36 = f32[1024,4096]{1,0:T(8,128)} fusion(bf16[1024,512]{0,1:T(8,128)(2,1)S(1)} %fusion.20, bf16[512,4096]{1,0:T(8,128)(2,1)} %all-gather.11.cloned.1.call-done), kind=kOutput, calls=%fused_computation.94 | convolution fusion | flops 4294967296 | bytes 22020096 | tf_op jit(solution)/shard_map/dot_general | solution.py:328
  392.8 38.8 %all-gather.21.cloned.1.call-done = bf16[32,128,256]{2,1,0:T(8,128)(2,1)} async-done(((bf16[4,128,256]{2,1,0:T(8,128)(2,1)}), bf16[32,128,256]{2,1,0:T(8,128)(2,1)}) %all-gather.21.cloned.1.call-update) | async-done | bytes 2097168 | tf_op jit(solution)/shard_map/all_gather | solution.py:310
  431.6 6.2 %shard_map.173 = bf16[1024,512]{1,0:T(8,128)(2,1)} custom-call(s32[1]{0:T(128)} %bitcast.2.place_ref, bf16[8,4,128,256]{3,2,1,0:T(8,128)(2,1)} %bitcast.34, f32[1024,512]{1,0:T(8,128)} %get-tuple-element.9.local_ref, bf16[1024,512]{1,0:T(8,128)(2,1)} %get-tuple-element.10.reach_ref, bf16[1,128]{1,0:T(2,128)(2,1)} %bitcast.36), custom_call_target="tpu_custom_call" | custom-call | flops 268435456 | bytes 4194304 | tf_op jit(solution)/shard_map/pallas_call | solution.py:216
  437.8 69.0 %all-gather.19.cloned.1.call-done = bf16[512,4096]{1,0:T(8,128)(2,1)} async-done(((bf16[512,512]{1,0:T(8,128)(2,1)}), bf16[512,4096]{1,0:T(8,128)(2,1)}) %all-gather.19.cloned.1.call-update) | async-done | bytes 4194320 | tf_op jit(solution)/shard_map/all_gather | solution.py:335
  506.8 15.2 %add_convert_fusion = bf16[1024,4096]{1,0:T(8,128)(2,1)} fusion(f32[1024,4096]{1,0:T(8,128)} %fusion.36, bf16[1024,512]{1,0:T(8,128)(2,1)} %shard_map.173, bf16[512,4096]{1,0:T(8,128)(2,1)} %all-gather.19.cloned.1.call-done), kind=kOutput, calls=%fused_computation.5 | convolution fusion | flops 4303355904 | bytes 30408704 | tf_op jit(solution)/shard_map/dot_general | solution.py:333
  522.0 0.0 reduce-scatter.2.cloned.1.call-update
  522.0 69.8 %reduce-scatter.2.cloned.1.call-done = bf16[256,4096]{1,0:T(8,128)(2,1)} async-done(((bf16[1024,4096]{1,0:T(8,128)(2,1)}), bf16[256,4096]{1,0:T(8,128)(2,1)}) %reduce-scatter.2.cloned.1.call-update) | async-done | bytes 2097168 | tf_op jit(solution)/shard_map/reduce_scatter | solution.py:338
  (28 shorter events, 0.2 us)
Async XLA Ops:
  6.5 313.7 %copy-start = (bf16[16,128,128]{2,1,0:T(8,128)(2,1)S(1)}, bf16[16,128,128]{2,1,0:T(8,128)(2,1)}, u32[]{:S(2)}) copy-start(bf16[16,128,128]{2,1,0:T(8,128)(2,1)} %param.32) | copy-start | bytes 1572868
  6.5 3.4 copy-start.4
  6.5 79.0 %all-gather.17.cloned.1.call-start = ((), (), s32[]{:S(2)}) async-start(), calls=%async_computation.5 | async-start | bytes 4718592 | tf_op jit(solution)/shard_map/all_gather | solution.py:271
  7.3 151.9 %all-gather.15.cloned.1.call-start = ((), (), s32[]{:S(2)}) async-start(), calls=%async_computation.4 | async-start | bytes 4718592 | tf_op jit(solution)/shard_map/all_gather | solution.py:271
  8.0 224.7 %all-gather.13.cloned.1.call-start = ((), (), s32[]{:S(2)}) async-start(), calls=%async_computation.3 | async-start | bytes 4718592 | tf_op jit(solution)/shard_map/all_gather | solution.py:271
  8.7 297.9 %all-gather.9.cloned.1.call-start = ((), (), s32[]{:S(2)}) async-start(), calls=%async_computation.1 | async-start | bytes 4718592 | tf_op jit(solution)/shard_map/all_gather | solution.py:280
  9.3 372.9 %all-gather.11.cloned.1.call-start = ((), (), s32[]{:S(2)}) async-start(), calls=%async_computation.2 | async-start | bytes 4718592 | tf_op jit(solution)/shard_map/all_gather | solution.py:330
  9.9 421.6 %all-gather.21.cloned.1.call-start = ((), (), s32[]{:S(2)}) async-start(), calls=%async_computation.8 | async-start | bytes 2359296 | tf_op jit(solution)/shard_map/all_gather | solution.py:310
  15.1 10.5 %copy-start.8 = (f32[16]{0:T(128)S(1)}, f32[16]{0:T(128)}, u32[]{:S(2)}) copy-start(f32[16]{0:T(128)} %param.28) | copy-start | bytes 196
  15.1 10.6 %copy-start.9 = (f32[16]{0:T(128)S(1)}, f32[16]{0:T(128)}, u32[]{:S(2)}) copy-start(f32[16]{0:T(128)} %param.29) | copy-start | bytes 196
  15.1 10.6 %copy-start.5 = (bf16[512,4]{0,1:T(4,128)(2,1)S(1)}, bf16[512,4]{0,1:T(4,128)(2,1)}, u32[]{:S(2)}) copy-start(bf16[512,4]{0,1:T(4,128)(2,1)} %param.25) | copy-start | bytes 12292
  15.1 10.6 %copy-start.6 = (bf16[512,4]{0,1:T(4,128)(2,1)S(1)}, bf16[512,4]{0,1:T(4,128)(2,1)}, u32[]{:S(2)}) copy-start(bf16[512,4]{0,1:T(4,128)(2,1)} %param.24) | copy-start | bytes 12292
  15.1 44.2 %copy-start.10 = (f32[16]{0:T(128)S(1)}, f32[16]{0:T(128)}, u32[]{:S(2)}) copy-start(f32[16]{0:T(128)} %param.27) | copy-start | bytes 196
  59.3 5.7 copy-start.3
  242.0 1.6 copy-start.2
  243.7 5.1 collective-permute-start.1
  248.7 0.6 copy-start.7
  280.1 226.7 %all-gather.19.cloned.1.call-start = ((), (), s32[]{:S(2)}) async-start(), calls=%async_computation.6 | async-start | bytes 4718592 | tf_op jit(solution)/shard_map/all_gather | solution.py:335
  280.8 310.9 %reduce-scatter.2.cloned.1.call-start = ((), (), s32[]{:S(2)}) async-start(), calls=%async_computation.7 | async-start | bytes 10485760 | tf_op jit(solution)/shard_map/reduce_scatter | solution.py:338
  315.7 4.2 collective-permute-start
  522.0 69.8 %copy-start.1 = (bf16[16,128,128]{2,1,0:T(8,128)(2,1)S(1)}, bf16[16,128,128]{2,1,0:T(8,128)(2,1)}, u32[]{:S(2)}) copy-start(bf16[16,128,128]{2,1,0:T(8,128)(2,1)} %param.32) | copy-start | bytes 1572868
Sparse Core Ops, SparseCore 0:
  9.5 76.0 all-gather.16
  87.7 71.4 all-gather.14
  161.3 71.3 all-gather.12
  234.7 71.9 all-gather.8
  308.6 73.6 all-gather.10
  384.3 47.2 all-gather.20
  433.6 73.1 all-gather.18
  522.1 69.5 reduce-scatter.1
